TPU v7x, 256 devices: a whole 4x4x8 slice. The times are simulated.
256 devices in a mesh: ep: 64 (over z, y, core), tp: 4 (over x).
Axes of the slice: x: 4, y: 4, z: 8, core: 2. Of those that a mesh axis runs over, the one named last changes fastest.
Arguments:
- mixer_in: bfloat16 [24576, 2048], P(('ep', 'tp')), may hold values from -6 to 6
- expert_in: bfloat16 [24576, 2048], P(('ep', 'tp')), may hold values from -6 to 6
- mixer_gain: float32 [2048], replicated, may hold values from 0.1 to 1.9
- in_gate_weight: bfloat16 [2048, 2048], P(None, 'tp'), may hold values from -0.125 to 0.125
- out_gate_weight: bfloat16 [2048, 2048], P(None, 'tp'), may hold values from -0.125 to 0.125
- value_weight: bfloat16 [2048, 2048], P(None, 'tp'), may hold values from -0.125 to 0.125
- conv_taps: float32 [3, 2048], replicated, may hold values from -3 to 3
- mixer_proj: bfloat16 [2048, 2048], P(None, 'tp'), may hold values from -0.125 to 0.125
- expert_gain: float32 [2048], replicated, may hold values from 0.1 to 1.9
- route_ids: int32 [24576, 2], P('ep'), may hold values from 0 to 63, all different within a row; in each aligned block of 96 rows (0 to 95, 96 to 191, ...) at most 6 rows name the same one
- route_weights: float32 [24576, 2], P('ep'), may hold values from 0.1 to 1
- gate_weight: bfloat16 [64, 2048, 1024], P('ep', None, 'tp'), may hold values from -0.125 to 0.125
- up_weight: bfloat16 [64, 2048, 1024], P('ep', None, 'tp'), may hold values from -0.125 to 0.125
- down_weight: bfloat16 [64, 1024, 2048], P('ep', None, 'tp'), may hold values from -0.1875 to 0.1875
Outputs:
- mixer_out: bfloat16 [24576, 2048], P('ep', 'tp')
- expert_out: bfloat16 [24576, 2048], P('ep', 'tp')
Inputs may be any that keep to these rules, and one draw needn't show every extreme that they name: `route_ids`: each row names 2 different experts. In each aligned block of 96 rows no expert is named by more than 6 rows, a bound that some block reaches.
All inputs are finite; a program needn't handle non-finite values.
Results may differ from a plain program's by a relative error of at most 0.0076.
Values may be sent and summed in bfloat16 or wider, within the bound.
A program may use at most 64 MiB of HBM per device.

v0:
```python
import jax
import jax.numpy as jnp
from jax import lax
from jax.sharding import PartitionSpec as P

norm_eps = 1e-06


def sent_to_all(x, axis):
    peers = lax.axis_size(axis)
    return lax.all_to_all(jnp.broadcast_to(x[None], (peers, *x.shape)), axis, 0, 0, tiled=True)


def joined_along(tiles, dim):
    tiles = jnp.moveaxis(tiles, 0, dim)
    dims = tiles.shape
    return tiles.reshape(*dims[:dim], dims[dim] * dims[dim + 1], *dims[dim + 2 :])


def collect(x, axis, dim):
    tiles = sent_to_all(x, axis)
    return joined_along(tiles, dim)


def passed_along(value, axis, steps):
    count = lax.axis_size(axis)
    leading, last = (max(0, -steps), min(count, count - steps))
    return lax.ppermute(value, axis, [(source, source + steps) for source in range(leading, last)])


def rms_rows(values, gain_row):
    wide = values.astype(jnp.float32)
    scale = lax.rsqrt(jnp.mean(wide * wide, axis=-1, keepdims=True) + norm_eps)
    return (wide * scale * gain_row).astype(jnp.bfloat16)


def place_slots(route_ids, group_rows, experts, slot_cap):
    row_total, top_count = route_ids.shape
    groups = row_total // group_rows
    labels = jnp.arange(experts, dtype=jnp.int32)
    onehot = (
        route_ids.reshape(groups, group_rows * top_count)[:, :, None] == labels[None, None, :]
    ).astype(jnp.int32)
    earlier = jnp.cumsum(onehot, axis=1) - onehot
    within = jnp.sum(earlier * onehot, axis=2)
    slot_index = jnp.arange(groups, dtype=jnp.int32)[:, None] * slot_cap + within
    return slot_index.reshape(row_total, top_count)


def on_device(
    mixer_in,
    expert_in,
    mixer_gain,
    in_gate_weight,
    out_gate_weight,
    value_weight,
    conv_taps,
    mixer_proj,
    expert_gain,
    route_ids,
    route_weights,
    gate_weight,
    up_weight,
    down_weight,
):
    tok_dev = mixer_in.shape[0]
    tp_count = lax.axis_size("tp")
    ep_count = lax.axis_size("ep")
    top_count = route_ids.shape[1]
    experts = ep_count * gate_weight.shape[0]
    slot_cap = max(2, 2 * tok_dev * top_count // experts)
    tp_index = lax.axis_index("tp")
    mixer_normed = rms_rows(mixer_in, mixer_gain)
    expert_normed = rms_rows(expert_in, expert_gain)
    block_slot = place_slots(route_ids, tok_dev, experts, slot_cap)
    mixer_rows = collect(mixer_normed, "tp", 0)
    send_ids = lax.dynamic_slice_in_dim(route_ids, tp_index * tok_dev, tok_dev, 0)
    send_slot = (
        lax.dynamic_slice_in_dim(block_slot, tp_index * tok_dev, tok_dev, 0) - tp_index * slot_cap
    )
    source_count = expert_normed.shape[0]
    flat_index = (send_ids * slot_cap + send_slot).reshape(-1)
    row_table = (
        jnp.full((experts * slot_cap,), source_count, jnp.int32)
        .at[flat_index]
        .set(jnp.repeat(jnp.arange(source_count, dtype=jnp.int32), top_count))
    )
    padded_rows = jnp.concatenate(
        [expert_normed, jnp.zeros((1, expert_normed.shape[1]), jnp.bfloat16)], axis=0
    )
    outgoing = padded_rows[row_table].reshape(experts, slot_cap, expert_normed.shape[1])
    arrived = lax.all_to_all(outgoing, "ep", split_axis=0, concat_axis=0, tiled=True)
    arrived = lax.all_gather(arrived, "tp", axis=1, tiled=True)
    chan_width = in_gate_weight.shape[1]
    in_gate = jnp.dot(mixer_rows, in_gate_weight, preferred_element_type=jnp.float32)
    out_gate = jnp.dot(mixer_rows, out_gate_weight, preferred_element_type=jnp.float32)
    values = jnp.dot(mixer_rows, value_weight, preferred_element_type=jnp.float32)
    product = (in_gate * values).astype(jnp.bfloat16)
    tap_count = conv_taps.shape[0]
    rim_rows = passed_along(product[product.shape[0] - (tap_count - 1) :], "ep", 1)
    extended = jnp.concatenate([rim_rows, product], axis=0).astype(jnp.float32)
    tap_rows = lax.dynamic_slice_in_dim(conv_taps, tp_index * chan_width, chan_width, 1)
    row_count = product.shape[0]
    conv_sum = tap_rows[0] * extended[0:row_count]
    for tap_index in range(1, tap_count):
        conv_sum = conv_sum + tap_rows[tap_index] * extended[tap_index : tap_index + row_count]
    gated = (out_gate * conv_sum).astype(jnp.bfloat16)
    slots_in = arrived.reshape(-1, arrived.shape[2])
    gate_pre = jnp.dot(slots_in, gate_weight[0], preferred_element_type=jnp.float32)
    up_pre = jnp.dot(slots_in, up_weight[0], preferred_element_type=jnp.float32)
    hidden = (jax.nn.silu(gate_pre) * up_pre).astype(jnp.bfloat16)
    down_slice = down_weight[0]
    rows_part = mixer_proj
    mixer_sum = jnp.dot(
        lax.all_gather(gated, "tp", axis=1, tiled=True),
        rows_part,
        preferred_element_type=jnp.float32,
    )
    rows_part = down_slice
    expert_sum = jnp.dot(
        lax.all_gather(hidden, "tp", axis=1, tiled=True),
        rows_part,
        preferred_element_type=jnp.float32,
    )
    mixer_out = mixer_sum.astype(jnp.bfloat16)
    results = expert_sum.astype(jnp.bfloat16).reshape(ep_count, -1, expert_sum.shape[1])
    returned = lax.all_to_all(results, "ep", split_axis=0, concat_axis=0, tiled=True)
    back_index = (route_ids * (tp_count * slot_cap) + block_slot).reshape(-1)
    picked = returned.reshape(-1, returned.shape[2])[back_index].reshape(
        route_ids.shape[0], top_count, -1
    )
    shares = route_weights / jnp.sum(route_weights, axis=1, keepdims=True)
    expert_out = jnp.sum(picked.astype(jnp.float32) * shares[:, :, None], axis=1).astype(
        jnp.bfloat16
    )
    return (mixer_out, expert_out)


def solution(mesh):
    return jax.shard_map(
        on_device,
        mesh=mesh,
        in_specs=(
            P(("ep", "tp"), None),
            P(("ep", "tp"), None),
            P(),
            P(None, "tp"),
            P(None, "tp"),
            P(None, "tp"),
            P(),
            P(None, "tp"),
            P(),
            P("ep", None),
            P("ep", None),
            P("ep", None, "tp"),
            P("ep", None, "tp"),
            P("ep", None, "tp"),
        ),
        out_specs=(P("ep", "tp"), P("ep", "tp")),
        check_vma=False,
    )
```

profile of v0, /device:TPU:1, one launch (start us, length us, event | category | flops | bytes accessed | tf_op | source)
XLA Modules:
  0.0 291.8 jit_solution(16893624878074087516)
XLA Ops:
  7.2 1.0 copy.47
  8.2 0.1 eq.22
  8.5 2.4 reduce-window.6
  10.9 0.1 slice.48
  11.0 0.1 copy.49
  11.2 0.1 bitcast_bitcast_fusion
  11.4 0.2 reduce_sum.50
  11.6 0.1 copy.52
  11.7 0.1 add.93
  11.9 0.1 copy.53
  12.0 0.1 reshape.131
  12.2 0.1 reshape.160
  12.3 1.2 scatter_custom_fusion
  13.6 0.2 fusion.10
  13.8 0.2 fusion.12
  14.0 3.1 %gather_fusion = bf16[384,2048]{1,0:T(8,128)(2,1)} fusion(bf16[97,2048]{1,0:T(8,128)(2,1)S(1)} %concatenate.7, s32[1024]{0:T(1024)S(1)} %pad_clamp_fusion.1), kind=kCustom, calls=%fused_computation | custom fusion | bytes 3147264 | tf_op jit(solution)/shard_map/gather | solution.py:91
  17.1 3.7 %reshape.133 = bf16[64,6,2048]{2,1,0:T(8,128)(2,1)} reshape(bf16[384,2048]{1,0:T(8,128)(2,1)} %gather_fusion) | data formatting | bytes 3145728 | tf_op jit(solution)/shard_map/reshape | solution.py:91
  20.8 62.8 %all_to_all.15 = bf16[64,6,2048]{2,1,0:T(8,128)(2,1)S(1)} all-to-all(bf16[64,6,2048]{2,1,0:T(8,128)(2,1)} %reshape.133), channel_id=1, replica_groups=mesh['ep'=64,'tp'=4] {'ep'}, dimensions={0} | all-to-all | bytes 3145728 | tf_op jit(solution)/shard_map/all_to_all | solution.py:92
  83.6 2.0 copy.54
  85.7 0.2 all-gather.8.cloned.1.call-start
  85.9 65.5 %all-gather.6.cloned.1.call-done = bf16[64,24,2048]{2,0,1:T(8,128)(2,1)} async-done(((bf16[64,6,2048]{2,0,1:T(8,128)(2,1)}), bf16[64,24,2048]{2,0,1:T(8,128)(2,1)}) %all-gather.6.cloned.1.call-update) | async-done | bytes 6291472 | tf_op jit(solution)/shard_map/all_gather | solution.py:93
  151.4 6.2 %copy.55 = bf16[64,24,2048]{2,1,0:T(8,128)(2,1)S(1)} copy(bf16[64,24,2048]{2,0,1:T(8,128)(2,1)} %all-gather.6.cloned.1.call-done) | data formatting | bytes 12582912 | tf_op jit(solution)/shard_map/all_gather | solution.py:93
  157.7 3.2 %fusion.5 = f32[1536,256]{1,0:T(8,128)S(1)} fusion(bf16[1536,2048]{1,0:T(8,128)(2,1)S(1)} %bitcast.43, bf16[1,2048,256]{2,1,0:T(8,128)(2,1)} %param.25), kind=kOutput, calls=%fused_computation.14 | convolution fusion | flops 1610612736 | bytes 8912896 | tf_op jit(solution)/shard_map/dot_general | solution.py:109
  160.9 3.0 %fusion = bf16[1536,256]{1,0:T(8,128)(2,1)} fusion(bf16[1536,2048]{1,0:T(8,128)(2,1)S(1)} %bitcast.44, f32[1536,256]{1,0:T(8,128)S(1)} %fusion.5, bf16[1,2048,256]{2,1,0:T(8,128)(2,1)S(1)} %copy-done.8), kind=kOutput, calls=%fused_computation.5 | convolution fusion | flops 1612972032 | bytes 9699328 | tf_op jit(solution)/shard_map/dot_general | solution.py:110
  163.9 0.2 fusion.7
  164.1 0.2 fusion.9
  164.3 1.4 broadcast_in_dim.8
  165.6 4.3 %all-to-all-start = ((bf16[4,96,2048]{2,1,0:T(8,128)(2,1)}), bf16[4,96,2048]{2,1,0:T(8,128)(2,1)}, u32[]{:S(2)}, u32[]{:S(2)}) async-start(bf16[4,96,2048]{2,1,0:T(8,128)(2,1)} %broadcast_in_dim.8), calls=%async_computation | async-start | bytes 3145728 | tf_op jit(solution)/shard_map/all_to_all | solution.py:11
  170.0 28.0 %all-to-all-done = bf16[4,96,2048]{2,1,0:T(8,128)(2,1)} async-done(((bf16[4,96,2048]{2,1,0:T(8,128)(2,1)}), bf16[4,96,2048]{2,1,0:T(8,128)(2,1)}, u32[]{:S(2)}, u32[]{:S(2)}) %all-to-all-start) | async-done | bytes 1572896 | tf_op jit(solution)/shard_map/all_to_all | solution.py:11
  198.0 2.5 fusion.22
  200.6 2.4 fusion.2
  203.0 5.1 %collective-permute-start = (bf16[2,512]{1,0:T(2,128)(2,1)S(1)}, bf16[2,512]{1,0:T(2,128)(2,1)S(1)}, u32[]{:S(2)}, u32[]{:S(2)}) collective-permute-start(bf16[2,512]{1,0:T(2,128)(2,1)S(1)} %slice.44), channel_id=1, source_target_pairs={{0,4},{4,8},{8,12},{12,16},{16,20},{20,24},{24,28},{28,32},{32,36}... | collective-permute-start | bytes 6152 | tf_op jit(solution)/shard_map/ppermute | solution.py:28
  208.2 0.9 constant_dynamic-slice_fusion
  209.1 0.1 maximum_convert_fusion
  209.2 8.7 %all-gather.8.cloned.1.call-done = bf16[1536,1024]{1,0:T(8,128)(2,1)} async-done(((bf16[1536,256]{1,0:T(8,128)(2,1)}), bf16[1536,1024]{1,0:T(8,128)(2,1)}) %all-gather.8.cloned.1.call-update) | async-done | bytes 3145744 | tf_op jit(solution)/shard_map/all_gather | solution.py:121
  217.8 5.1 %convolution_convert_fusion = bf16[1536,512]{1,0:T(8,128)(2,1)} fusion(bf16[1536,1024]{1,0:T(8,128)(2,1)} %all-gather.8.cloned.1.call-done, bf16[1,1024,512]{2,1,0:T(8,128)(2,1)} %param.27), kind=kOutput, calls=%fused_computation.3 | convolution fusion | flops 1611399168 | bytes 5767168 | tf_op jit(solution)/shard_map/dot_general | solution.py:120
  223.0 12.5 %all-to-all-start.2 = ((bf16[64,24,512]{2,1,0:T(8,128)(2,1)}), bf16[64,24,512]{2,1,0:T(8,128)(2,1)}, u32[]{:S(2)}, u32[]{:S(2)}) async-start(bf16[64,24,512]{2,1,0:T(8,128)(2,1)} %bitcast.45), calls=%async_computation.2 | async-start | bytes 3145728 | tf_op jit(solution)/shard_map/all_to_all | solution.py:127
  235.5 0.3 all-gather.4.cloned.1.call-start
  235.7 3.9 %fusion.1 = bf16[384,512]{1,0:T(8,128)(2,1)} fusion(bf16[384,2048]{1,0:T(8,128)(2,1)} %bitcast, bf16[2048,512]{1,0:T(8,128)(2,1)} %param.18, f32[386,512]{1,0:T(8,128)S(1)} %maximum_convert_fusion, f32[512]{0:T(512)S(1)} %bitcast.48, f32[512]{0:T(512)S(1)} %bitcast.47, f32[512]{0:T(512)S(1)} %bitcast.46), kind=kOutput, calls=%fused_computation.9 | convolution fusion | flops 806682624 | bytes 6428672 | tf_op jit(solution)/shard_map/dot_general | solution.py:96
  239.7 0.1 copy.56
  239.8 0.2 reshape.137
  240.0 0.1 copy.57
  240.2 28.4 %all-gather.4.cloned.1.call-done = bf16[384,2048]{1,0:T(8,128)(2,1)} async-done(((bf16[384,512]{1,0:T(8,128)(2,1)}), bf16[384,2048]{1,0:T(8,128)(2,1)}) %all-gather.4.cloned.1.call-update) | async-done | bytes 1572880 | tf_op jit(solution)/shard_map/all_gather | solution.py:115
  268.6 3.8 %convolution_convert_fusion.1 = bf16[384,512]{1,0:T(8,128)(2,1)} fusion(bf16[384,2048]{1,0:T(8,128)(2,1)} %all-gather.4.cloned.1.call-done, bf16[2048,512]{1,0:T(8,128)(2,1)} %param.21), kind=kOutput, calls=%fused_computation.11 | convolution fusion | flops 805502976 | bytes 4063232 | tf_op jit(solution)/shard_map/dot_general | solution.py:114
  272.4 2.1 all-to-all-done.2
  274.5 4.3 %gather_fusion.1 = bf16[768,512]{1,0:T(8,128)(2,1)S(1)} fusion(bf16[1536,512]{1,0:T(8,128)(2,1)} %bitcast.12, s32[1024]{0:T(1024)S(1)} %pad_clamp_fusion), kind=kCustom, calls=%fused_computation.1 | custom fusion | bytes 1575936 | tf_op jit(solution)/shard_map/gather | solution.py:129
  278.8 2.1 reshape.139
  280.9 4.3 %multiply_reduce_fusion = bf16[384,512]{1,0:T(8,128)(2,1)} fusion(f32[384,2,512]{2,1,0:T(2,128)} %reshape.139, f32[384,2]{1,0:T(8,128)S(1)} %copy.57), kind=kLoop, calls=%fused_computation.6 | loop fusion | flops 589824 | bytes 1969152 | tf_op jit(solution)/shard_map/reduce_sum | solution.py:133
  (45 shorter events, 0.6 us)
Async XLA Ops:
  7.2 190.8 %copy-start = (bf16[2048,512]{1,0:T(8,128)(2,1)S(1)}, bf16[2048,512]{1,0:T(8,128)(2,1)}, u32[]{:S(2)}) copy-start(bf16[2048,512]{1,0:T(8,128)(2,1)} %param.17) | copy-start | bytes 6291460
  7.2 144.2 %all-gather.6.cloned.1.call-start = ((), (), s32[]{:S(2)}) async-start(), calls=%async_computation.4 | async-start | bytes 7864320 | tf_op jit(solution)/shard_map/all_gather | solution.py:93
  8.2 3.6 %copy-start.3 = (s32[384,2]{0,1:T(2,128)S(1)}, s32[384,2]{0,1:T(2,128)}, u32[]{:S(2)}) copy-start(s32[384,2]{0,1:T(2,128)} %param.23) | copy-start | bytes 9220
  8.4 5.1 %copy-start.1 = (bf16[96,2048]{1,0:T(8,128)(2,1)S(1)}, bf16[96,2048]{1,0:T(8,128)(2,1)}, u32[]{:S(2)}) copy-start(bf16[96,2048]{1,0:T(8,128)(2,1)} %param.15) | copy-start | bytes 1179652
  8.5 5.3 %copy-start.5 = (f32[2048]{0:T(1024)S(1)}, f32[2048]{0:T(1024)}, u32[]{:S(2)}) copy-start(f32[2048]{0:T(1024)} %param.22) | copy-start | bytes 24580
  85.7 132.2 %all-gather.8.cloned.1.call-start = ((), (), s32[]{:S(2)}) async-start(), calls=%async_computation.5 | async-start | bytes 3932160 | tf_op jit(solution)/shard_map/all_gather | solution.py:121
  157.6 3.2 %copy-start.8 = (bf16[1,2048,256]{2,1,0:T(8,128)(2,1)S(1)}, bf16[1,2048,256]{2,1,0:T(8,128)(2,1)}, u32[]{:S(2)}) copy-start(bf16[1,2048,256]{2,1,0:T(8,128)(2,1)} %param.26) | copy-start | bytes 3145732
  160.9 3.0 %copy-start.2 = (bf16[96,2048]{1,0:T(8,128)(2,1)S(1)}, bf16[96,2048]{1,0:T(8,128)(2,1)}, u32[]{:S(2)}) copy-start(bf16[96,2048]{1,0:T(8,128)(2,1)} %param.14) | copy-start | bytes 1179652
  160.9 3.2 %copy-start.6 = (f32[2048]{0:T(1024)S(1)}, f32[2048]{0:T(1024)}, u32[]{:S(2)}) copy-start(f32[2048]{0:T(1024)} %param.16) | copy-start | bytes 24580
  165.6 32.4 %all-to-all-start = ((bf16[4,96,2048]{2,1,0:T(8,128)(2,1)}), bf16[4,96,2048]{2,1,0:T(8,128)(2,1)}, u32[]{:S(2)}, u32[]{:S(2)}) async-start(bf16[4,96,2048]{2,1,0:T(8,128)(2,1)} %broadcast_in_dim.8), calls=%async_computation | async-start | bytes 3145728 | tf_op jit(solution)/shard_map/all_to_all | solution.py:11
  198.0 2.6 copy-start.7
  203.0 6.0 %collective-permute-start = (bf16[2,512]{1,0:T(2,128)(2,1)S(1)}, bf16[2,512]{1,0:T(2,128)(2,1)S(1)}, u32[]{:S(2)}, u32[]{:S(2)}) collective-permute-start(bf16[2,512]{1,0:T(2,128)(2,1)S(1)} %slice.44), channel_id=1, source_target_pairs={{0,4},{4,8},{8,12},{12,16},{16,20},{20,24},{24,28},{28,32},{32,36}... | collective-permute-start | bytes 6152 | tf_op jit(solution)/shard_map/ppermute | solution.py:28
  223.0 51.5 %all-to-all-start.2 = ((bf16[64,24,512]{2,1,0:T(8,128)(2,1)}), bf16[64,24,512]{2,1,0:T(8,128)(2,1)}, u32[]{:S(2)}, u32[]{:S(2)}) async-start(bf16[64,24,512]{2,1,0:T(8,128)(2,1)} %bitcast.45), calls=%async_computation.2 | async-start | bytes 3145728 | tf_op jit(solution)/shard_map/all_to_all | solution.py:127
  235.5 33.1 %all-gather.4.cloned.1.call-start = ((), (), s32[]{:S(2)}) async-start(), calls=%async_computation.3 | async-start | bytes 1966080 | tf_op jit(solution)/shard_map/all_gather | solution.py:115
  235.7 4.2 %copy-start.4 = (f32[384,2]{0,1:T(2,128)S(1)}, f32[384,2]{0,1:T(2,128)}, u32[]{:S(2)}) copy-start(f32[384,2]{0,1:T(2,128)} %param.24) | copy-start | bytes 9220
Sparse Core Ops, SparseCore 0:
  85.8 65.5 all-gather.5
  164.0 53.7 all-gather.7
  239.8 28.7 all-gather.3
where the time goes:
time: 292 us
  waiting for transfers between devices  133 us (46%)
  blocking collectives  62.8 us (22%)
  local copies, waits for them, and re-layouts  27.6 us (9%)
  matrix products  24 us (8%)
  starting transfers between devices  22.4 us (8%)
  between operations  14.1 us (5%)
  other arithmetic  8 us (3%)
    all_gather x1, waiting for transfers between devices, on_device(): arrived = lax.all_gather(arrived, 'tp', axis=1, tiled=True)  65.5 us
    all_to_all x1, blocking collectives, on_device(): lax.all_to_all(outgoing, 'ep', split_axis=0, concat_axis=0, tiled=True)  62.8 us
    all_gather x1, waiting for transfers between devices, on_device(): lax.all_gather(gated, 'tp', axis=1, tiled=True)  28.4 us
    all_to_all x1, waiting for transfers between devices, sent_to_all(): lax.all_to_all(jnp.broadcast_to(x[None], (peers, *x.shape)), axis, 0, 0,...  28 us
    all_to_all x1, starting transfers between devices, on_device(): lax.all_to_all(results, 'ep', split_axis=0, concat_axis=0, tiled=True)  12.5 us
    all_gather x1, waiting for transfers between devices, on_device(): lax.all_gather(hidden, 'tp', axis=1, tiled=True)  8.66 us
    all_gather x1, local copies, waits for them, and re-layouts, on_device(): arrived = lax.all_gather(arrived, 'tp', axis=1, tiled=True)  6.23 us
  transfers between devices with their start and end apart: 6, of which 5 were waited for; matrix products, arithmetic and copies ran while one was open for 5% of the time, Pallas kernels for 0%

commit v1 on v0

--- a/solution.py
+++ b/solution.py
@@ -90,7 +90,11 @@
     )
     outgoing = padded_rows[row_table].reshape(experts, slot_cap, expert_normed.shape[1])
     arrived = lax.all_to_all(outgoing, "ep", split_axis=0, concat_axis=0, tiled=True)
-    arrived = lax.all_gather(arrived, "tp", axis=1, tiled=True)
+    peers_2 = lax.axis_size("tp")
+    repeats = [peers_2 if d == 1 else 1 for d in range(arrived.ndim)]
+    arrived = lax.all_to_all(
+        jnp.tile(arrived, repeats), "tp", split_axis=1, concat_axis=1, tiled=True
+    )
     chan_width = in_gate_weight.shape[1]
     in_gate = jnp.dot(mixer_rows, in_gate_weight, preferred_element_type=jnp.float32)
     out_gate = jnp.dot(mixer_rows, out_gate_weight, preferred_element_type=jnp.float32)

time: 292 us -> 294 us (level)
  blocking collectives: 62.8 us -> 136 us
  waiting for transfers between devices: 133 us -> 66 us
  local copies, waits for them, and re-layouts: 27.6 us -> 24.5 us
    all_to_all x0 -> x1, blocking collectives: none -> 72.8 us  [on_device(): lax.all_to_all(jnp.tile(arrived, repeats), 'tp', split_axis=1, concat_axi...]
    all_gather x1 -> x0, waiting for transfers between devices: 65.5 us -> none  [on_device(): arrived = lax.all_gather(arrived, 'tp', axis=1, tiled=True)]
    all_gather x1 -> x0, local copies, waits for them, and re-layouts: 6.23 us -> none  [on_device(): arrived = lax.all_gather(arrived, 'tp', axis=1, tiled=True)]
    all_to_all x0 -> x1, local copies, waits for them, and re-layouts: none -> 3.45 us  [on_device(): lax.all_to_all(jnp.tile(arrived, repeats), 'tp', split_axis=1, concat_axi...]
  transfers between devices with their start and end apart: 6 -> 5, of which waited for: 5 -> 4; matrix products, arithmetic and copies ran while one was open for 5% -> 5% of each run, Pallas kernels for 0% -> 0%
where the time goes in v1:
time: 294 us; the launch traced here: 293 us
  blocking collectives  136 us (46%)
  waiting for transfers between devices  66 us (22%)
  local copies, waits for them, and re-layouts  24.5 us (8%)
  matrix products  22.7 us (8%)
  starting transfers between devices  21.8 us (7%)
  between operations  14.4 us (5%)
  other arithmetic  8 us (3%)
    all_to_all x1, blocking collectives, on_device(): lax.all_to_all(jnp.tile(arrived, repeats), 'tp', split_axis=1, concat_axi...  72.8 us
    all_to_all x1, blocking collectives, on_device(): lax.all_to_all(outgoing, 'ep', split_axis=0, concat_axis=0, tiled=True)  62.8 us
    all_gather x1, waiting for transfers between devices, on_device(): lax.all_gather(gated, 'tp', axis=1, tiled=True)  27.9 us
    all_to_all x1, waiting for transfers between devices, sent_to_all(): lax.all_to_all(jnp.broadcast_to(x[None], (peers, *x.shape)), axis, 0, 0,...  26 us
    all_to_all x1, starting transfers between devices, on_device(): lax.all_to_all(results, 'ep', split_axis=0, concat_axis=0, tiled=True)  10.1 us
    all_gather x1, waiting for transfers between devices, on_device(): lax.all_gather(hidden, 'tp', axis=1, tiled=True)  9.57 us
    ppermute x1, starting transfers between devices, passed_along(): lax.ppermute(value, axis, [(source, source + steps) for source in range(l...  7.02 us
  transfers between devices with their start and end apart: 5, of which 4 were waited for; matrix products, arithmetic and copies ran while one was open for 5% of the time, Pallas kernels for 0%

profile of v1, /device:TPU:1, one launch (start us, length us, event | category | flops | bytes accessed | tf_op | source)
XLA Modules:
  0.0 293.1 jit_solution(2805148648448951049)
XLA Ops:
  7.2 1.0 copy.38
  8.2 0.1 eq.22
  8.5 2.4 reduce-window.6
  10.9 0.1 slice.48
  11.0 0.1 copy.40
  11.2 0.1 bitcast_bitcast_fusion
  11.4 0.2 reduce_sum.50
  11.6 0.1 copy.43
  11.7 0.1 add.93
  11.9 0.1 copy.44
  12.0 0.1 reshape.135
  12.2 0.1 reshape.164
  12.3 1.2 scatter_custom_fusion
  13.6 0.2 fusion.10
  13.8 0.2 fusion.12
  14.0 3.1 %gather_fusion = bf16[384,2048]{1,0:T(8,128)(2,1)} fusion(bf16[97,2048]{1,0:T(8,128)(2,1)S(1)} %concatenate.7, s32[1024]{0:T(1024)S(1)} %pad_clamp_fusion.1), kind=kCustom, calls=%fused_computation | custom fusion | bytes 3147264 | tf_op jit(solution)/shard_map/gather | solution.py:91
  17.1 3.7 %reshape.137 = bf16[64,6,2048]{2,1,0:T(8,128)(2,1)} reshape(bf16[384,2048]{1,0:T(8,128)(2,1)} %gather_fusion) | data formatting | bytes 3145728 | tf_op jit(solution)/shard_map/reshape | solution.py:91
  20.8 62.8 %all_to_all.20 = bf16[64,6,2048]{2,1,0:T(8,128)(2,1)S(1)} all-to-all(bf16[64,6,2048]{2,1,0:T(8,128)(2,1)} %reshape.137), channel_id=1, replica_groups=mesh['ep'=64,'tp'=4] {'ep'}, dimensions={0} | all-to-all | bytes 3145728 | tf_op jit(solution)/shard_map/all_to_all | solution.py:92
  83.6 0.9 copy.45
  84.5 0.8 tile.4
  85.3 72.8 %all_to_all.21 = bf16[64,24,2048]{2,0,1:T(8,128)(2,1)S(1)} all-to-all(bf16[64,24,2048]{2,0,1:T(8,128)(2,1)S(1)} %bitcast.44), channel_id=1, replica_groups=mesh['ep'=64,'tp'=4] {'tp'}, dimensions={1} | all-to-all | bytes 12582912 | tf_op jit(solution)/shard_map/all_to_all | solution.py:95
  158.1 3.4 %copy.46 = bf16[64,24,2048]{2,1,0:T(8,128)(2,1)S(1)} copy(bf16[64,24,2048]{2,0,1:T(8,128)(2,1)S(1)} %all_to_all.21) | data formatting | bytes 12582912 | tf_op jit(solution)/shard_map/all_to_all | solution.py:95
  161.6 1.9 fusion.5
  163.5 3.0 %fusion = bf16[1536,256]{1,0:T(8,128)(2,1)} fusion(bf16[1536,2048]{1,0:T(8,128)(2,1)S(1)} %bitcast.46, f32[1536,256]{1,0:T(8,128)S(1)} %fusion.5, bf16[1,2048,256]{2,1,0:T(8,128)(2,1)S(1)} %copy-done.9), kind=kOutput, calls=%fused_computation.5 | convolution fusion | flops 1612972032 | bytes 9699328 | tf_op jit(solution)/shard_map/dot_general | solution.py:114
  166.5 0.2 fusion.7
  166.7 0.2 fusion.9
  166.9 1.4 broadcast_in_dim.8
  168.2 4.3 %all-to-all-start = ((bf16[4,96,2048]{2,1,0:T(8,128)(2,1)}), bf16[4,96,2048]{2,1,0:T(8,128)(2,1)}, u32[]{:S(2)}, u32[]{:S(2)}) async-start(bf16[4,96,2048]{2,1,0:T(8,128)(2,1)} %broadcast_in_dim.8), calls=%async_computation | async-start | bytes 3145728 | tf_op jit(solution)/shard_map/all_to_all | solution.py:11
  172.6 26.0 %all-to-all-done = bf16[4,96,2048]{2,1,0:T(8,128)(2,1)} async-done(((bf16[4,96,2048]{2,1,0:T(8,128)(2,1)}), bf16[4,96,2048]{2,1,0:T(8,128)(2,1)}, u32[]{:S(2)}, u32[]{:S(2)}) %all-to-all-start) | async-done | bytes 1572896 | tf_op jit(solution)/shard_map/all_to_all | solution.py:11
  198.6 2.6 fusion.22
  201.1 2.4 fusion.2
  203.6 7.0 %collective-permute-start = (bf16[2,512]{1,0:T(2,128)(2,1)S(1)}, bf16[2,512]{1,0:T(2,128)(2,1)S(1)}, u32[]{:S(2)}, u32[]{:S(2)}) collective-permute-start(bf16[2,512]{1,0:T(2,128)(2,1)S(1)} %slice.44), channel_id=1, source_target_pairs={{0,4},{4,8},{8,12},{12,16},{16,20},{20,24},{24,28},{28,32},{32,36}... | collective-permute-start | bytes 6152 | tf_op jit(solution)/shard_map/ppermute | solution.py:28
  210.6 0.9 constant_dynamic-slice_fusion
  211.5 0.1 maximum_convert_fusion
  211.6 9.6 %all-gather.5.cloned.1.call-done = bf16[1536,1024]{1,0:T(8,128)(2,1)} async-done(((bf16[1536,256]{1,0:T(8,128)(2,1)}), bf16[1536,1024]{1,0:T(8,128)(2,1)}) %all-gather.5.cloned.1.call-update) | async-done | bytes 3145744 | tf_op jit(solution)/shard_map/all_gather | solution.py:125
  221.2 5.1 %convolution_convert_fusion = bf16[1536,512]{1,0:T(8,128)(2,1)} fusion(bf16[1536,1024]{1,0:T(8,128)(2,1)} %all-gather.5.cloned.1.call-done, bf16[1,1024,512]{2,1,0:T(8,128)(2,1)} %param.27), kind=kOutput, calls=%fused_computation.3 | convolution fusion | flops 1611399168 | bytes 5767168 | tf_op jit(solution)/shard_map/dot_general | solution.py:124
  226.3 10.1 %all-to-all-start.3 = ((bf16[64,24,512]{2,1,0:T(8,128)(2,1)}), bf16[64,24,512]{2,1,0:T(8,128)(2,1)}, u32[]{:S(2)}, u32[]{:S(2)}) async-start(bf16[64,24,512]{2,1,0:T(8,128)(2,1)} %bitcast.47), calls=%async_computation.3 | async-start | bytes 3145728 | tf_op jit(solution)/shard_map/all_to_all | solution.py:131
  236.5 0.3 all-gather.3.cloned.1.call-start
  236.8 3.9 %fusion.1 = bf16[384,512]{1,0:T(8,128)(2,1)} fusion(bf16[384,2048]{1,0:T(8,128)(2,1)} %bitcast, bf16[2048,512]{1,0:T(8,128)(2,1)} %param.18, f32[386,512]{1,0:T(8,128)S(1)} %maximum_convert_fusion, f32[512]{0:T(512)S(1)} %bitcast.50, f32[512]{0:T(512)S(1)} %bitcast.49, f32[512]{0:T(512)S(1)} %bitcast.48), kind=kOutput, calls=%fused_computation.9 | convolution fusion | flops 806682624 | bytes 6428672 | tf_op jit(solution)/shard_map/dot_general | solution.py:100
  240.7 0.1 copy.47
  240.8 0.2 reshape.141
  241.1 0.1 copy.48
  241.2 27.9 %all-gather.3.cloned.1.call-done = bf16[384,2048]{1,0:T(8,128)(2,1)} async-done(((bf16[384,512]{1,0:T(8,128)(2,1)}), bf16[384,2048]{1,0:T(8,128)(2,1)}) %all-gather.3.cloned.1.call-update) | async-done | bytes 1572880 | tf_op jit(solution)/shard_map/all_gather | solution.py:119
  269.1 3.8 %convolution_convert_fusion.1 = bf16[384,512]{1,0:T(8,128)(2,1)} fusion(bf16[384,2048]{1,0:T(8,128)(2,1)} %all-gather.3.cloned.1.call-done, bf16[2048,512]{1,0:T(8,128)(2,1)} %param.21), kind=kOutput, calls=%fused_computation.11 | convolution fusion | flops 805502976 | bytes 4063232 | tf_op jit(solution)/shard_map/dot_general | solution.py:118
  272.9 2.6 all-to-all-done.3
  275.5 4.3 %gather_fusion.1 = bf16[768,512]{1,0:T(8,128)(2,1)S(1)} fusion(bf16[1536,512]{1,0:T(8,128)(2,1)} %bitcast.13, s32[1024]{0:T(1024)S(1)} %pad_clamp_fusion), kind=kCustom, calls=%fused_computation.1 | custom fusion | bytes 1575936 | tf_op jit(solution)/shard_map/gather | solution.py:133
  279.8 2.1 reshape.143
  281.9 4.3 %multiply_reduce_fusion = bf16[384,512]{1,0:T(8,128)(2,1)} fusion(f32[384,2,512]{2,1,0:T(2,128)} %reshape.143, f32[384,2]{1,0:T(8,128)S(1)} %copy.48), kind=kLoop, calls=%fused_computation.6 | loop fusion | flops 589824 | bytes 1969152 | tf_op jit(solution)/shard_map/reduce_sum | solution.py:137
  (46 shorter events, 0.6 us)
Async XLA Ops:
  7.2 191.4 %copy-start = (bf16[2048,512]{1,0:T(8,128)(2,1)S(1)}, bf16[2048,512]{1,0:T(8,128)(2,1)}, u32[]{:S(2)}) copy-start(bf16[2048,512]{1,0:T(8,128)(2,1)} %param.17) | copy-start | bytes 6291460
  7.2 214.0 %all-gather.5.cloned.1.call-start = ((), (), s32[]{:S(2)}) async-start(), calls=%async_computation.5 | async-start | bytes 3932160 | tf_op jit(solution)/shard_map/all_gather | solution.py:125
  8.2 3.6 %copy-start.3 = (s32[384,2]{0,1:T(2,128)S(1)}, s32[384,2]{0,1:T(2,128)}, u32[]{:S(2)}) copy-start(s32[384,2]{0,1:T(2,128)} %param.23) | copy-start | bytes 9220
  8.4 5.1 %copy-start.1 = (bf16[96,2048]{1,0:T(8,128)(2,1)S(1)}, bf16[96,2048]{1,0:T(8,128)(2,1)}, u32[]{:S(2)}) copy-start(bf16[96,2048]{1,0:T(8,128)(2,1)} %param.15) | copy-start | bytes 1179652
  8.4 5.3 %copy-start.5 = (f32[2048]{0:T(1024)S(1)}, f32[2048]{0:T(1024)}, u32[]{:S(2)}) copy-start(f32[2048]{0:T(1024)} %param.22) | copy-start | bytes 24580
  158.1 3.5 %copy-start.8 = (bf16[1,2048,256]{2,1,0:T(8,128)(2,1)S(1)}, bf16[1,2048,256]{2,1,0:T(8,128)(2,1)}, u32[]{:S(2)}) copy-start(bf16[1,2048,256]{2,1,0:T(8,128)(2,1)} %param.25) | copy-start | bytes 3145732
  161.6 1.9 copy-start.9
  163.5 3.0 %copy-start.2 = (bf16[96,2048]{1,0:T(8,128)(2,1)S(1)}, bf16[96,2048]{1,0:T(8,128)(2,1)}, u32[]{:S(2)}) copy-start(bf16[96,2048]{1,0:T(8,128)(2,1)} %param.14) | copy-start | bytes 1179652
  163.5 3.2 %copy-start.6 = (f32[2048]{0:T(1024)S(1)}, f32[2048]{0:T(1024)}, u32[]{:S(2)}) copy-start(f32[2048]{0:T(1024)} %param.16) | copy-start | bytes 24580
  168.2 30.3 %all-to-all-start = ((bf16[4,96,2048]{2,1,0:T(8,128)(2,1)}), bf16[4,96,2048]{2,1,0:T(8,128)(2,1)}, u32[]{:S(2)}, u32[]{:S(2)}) async-start(bf16[4,96,2048]{2,1,0:T(8,128)(2,1)} %broadcast_in_dim.8), calls=%async_computation | async-start | bytes 3145728 | tf_op jit(solution)/shard_map/all_to_all | solution.py:11
  198.6 2.6 copy-start.7
  203.6 7.9 %collective-permute-start = (bf16[2,512]{1,0:T(2,128)(2,1)S(1)}, bf16[2,512]{1,0:T(2,128)(2,1)S(1)}, u32[]{:S(2)}, u32[]{:S(2)}) collective-permute-start(bf16[2,512]{1,0:T(2,128)(2,1)S(1)} %slice.44), channel_id=1, source_target_pairs={{0,4},{4,8},{8,12},{12,16},{16,20},{20,24},{24,28},{28,32},{32,36}... | collective-permute-start | bytes 6152 | tf_op jit(solution)/shard_map/ppermute | solution.py:28
  226.3 49.2 %all-to-all-start.3 = ((bf16[64,24,512]{2,1,0:T(8,128)(2,1)}), bf16[64,24,512]{2,1,0:T(8,128)(2,1)}, u32[]{:S(2)}, u32[]{:S(2)}) async-start(bf16[64,24,512]{2,1,0:T(8,128)(2,1)} %bitcast.47), calls=%async_computation.3 | async-start | bytes 3145728 | tf_op jit(solution)/shard_map/all_to_all | solution.py:131
  236.5 32.6 %all-gather.3.cloned.1.call-start = ((), (), s32[]{:S(2)}) async-start(), calls=%async_computation.4 | async-start | bytes 1966080 | tf_op jit(solution)/shard_map/all_gather | solution.py:119
  236.8 4.2 %copy-start.4 = (f32[384,2]{0,1:T(2,128)S(1)}, f32[384,2]{0,1:T(2,128)}, u32[]{:S(2)}) copy-start(f32[384,2]{0,1:T(2,128)} %param.24) | copy-start | bytes 9220
Sparse Core Ops, SparseCore 0:
  166.6 54.5 all-gather.4
  240.8 28.2 all-gather.2
